TPU v7x, 128 devices: a whole 4x4x4 slice. The times are simulated.
128 devices in a mesh: sp: 16 (over z, y), tp: 8 (over x, core).
Axes of the slice: x: 4, y: 4, z: 4, core: 2. Of those that a mesh axis runs over, the one named last changes fastest.
Arguments:
- residual_in: bfloat16 [12288, 2048], P('sp', 'tp'), may hold values from -11 to 11
- queries: bfloat16 [12288, 1024], P('sp', 'tp'), may hold values from -6 to 6
- keys: bfloat16 [12288, 256], P('sp'), may hold values from -6 to 6
- values: bfloat16 [12288, 256], P('sp'), may hold values from -6 to 6
- query_gain: float32 [128], replicated, may hold values from 1.5 to 5
- key_norm_gain: float32 [128], replicated, may hold values from 1.5 to 5
- out_weight: bfloat16 [1024, 2048], P('tp'), may hold values from -0.1875 to 0.1875
- mlp_gain: float32 [2048], replicated, may hold values from 0.1 to 1.9
- gate_weight: bfloat16 [2048, 5632], P('sp', 'tp'), may hold values from -0.125 to 0.125
- up_weight: bfloat16 [2048, 5632], P('sp', 'tp'), may hold values from -0.125 to 0.125
- down_weight: bfloat16 [5632, 2048], P('tp', 'sp'), may hold values from -0.15625 to 0.15625
Outputs:
- layer_out: bfloat16 [12288, 2048], P('sp', 'tp')
All inputs are finite; a program needn't handle non-finite values.
Results may differ from a plain program's by a relative error of at most 0.012.
The roundings to bfloat16 on the way count: a program that leaves them out, or rounds other values in their place, can miss the bound.
Values may be sent and summed in bfloat16 or wider, within the bound.
A program may use at most 64 MiB of HBM per device.

v0:
```python
import jax
import jax.numpy as jnp
from jax import lax
from jax.sharding import PartitionSpec as P

D = 2048
HEAD_SIZE = 128
QUERY_HEADS = 8
KEY_VALUE_HEADS = 2
GRID = 64
eps = 1e-06
rotary_base = 10000.0


def sent_together(arrays, axis, dim, along):
    ends, at = ([], 0)
    for a in arrays[:-1]:
        at += a.shape[along]
        ends.append(at)
    both = jnp.concatenate(arrays, axis=along)
    return tuple(jnp.split(lax.all_gather(both, axis, axis=dim, tiled=True), ends, axis=along))


def laid_out(tiles, dim):
    tiles = jnp.moveaxis(tiles, 0, dim)
    lengths = tiles.shape
    return tiles.reshape(*lengths[:dim], lengths[dim] * lengths[dim + 1], *lengths[dim + 2 :])


def sent_to_all(x, axis):
    size = lax.axis_size(axis)
    return lax.all_to_all(jnp.broadcast_to(x[None], (size, *x.shape)), axis, 0, 0, tiled=True)


def gathered_copies(x, axis, dim):
    return laid_out(sent_to_all(x, axis), dim)


def taken_together(x, axis):
    everything = sent_to_all(x, axis)
    return jnp.sum(everything, axis=0)


def in_blocks(x, dim, size):
    lengths = x.shape
    tiles = x.reshape(*lengths[:dim], size, lengths[dim] // size, *lengths[dim + 1 :])
    return jnp.moveaxis(tiles, dim, 0)


def summed_on_arrival(x, axis, dim):
    tiles = in_blocks(x, dim, lax.axis_size(axis))
    arrived = lax.all_to_all(tiles, axis, split_axis=0, concat_axis=0, tiled=True)
    return arrived.astype(jnp.float32).sum(axis=0)


def apply_rotary(vectors, grid_positions):
    half_size = vectors.shape[-1] // 2
    frequency = rotary_base ** (-jnp.arange(0, half_size, 2, dtype=jnp.float32) / half_size)
    grid_row = (grid_positions // GRID).astype(jnp.float32)
    grid_col = (grid_positions % GRID).astype(jnp.float32)
    angles = jnp.concatenate(
        [grid_row[:, None] * frequency, grid_col[:, None] * frequency], axis=-1
    )[:, None, :]
    cosine_table = jnp.cos(angles)
    sine_table = jnp.sin(angles)
    first_half = vectors[..., :half_size]
    second_half = vectors[..., half_size:]
    return jnp.concatenate(
        [
            first_half * cosine_table - second_half * sine_table,
            first_half * sine_table + second_half * cosine_table,
        ],
        axis=-1,
    )


def per_head_norm(vectors, gain):
    return vectors * lax.rsqrt(jnp.mean(vectors * vectors, axis=-1, keepdims=True) + eps) * gain


def on_device(
    residual_in,
    queries,
    keys,
    values,
    query_gain,
    key_norm_gain,
    out_weight,
    mlp_gain,
    gate_weight,
    up_weight,
    down_weight,
):
    local_rows = residual_in.shape[0]
    local_heads = queries.shape[1] // HEAD_SIZE
    queries_per_group = QUERY_HEADS // KEY_VALUE_HEADS
    tp_index = lax.axis_index("tp")
    tp_count = lax.axis_size("tp")
    grid_positions = lax.axis_index("sp") * local_rows + jnp.arange(local_rows, dtype=jnp.int32)
    weight_cols = lax.all_to_all(out_weight, "tp", split_axis=1, concat_axis=0, tiled=True)
    query_rows = apply_rotary(
        per_head_norm(
            queries.astype(jnp.float32).reshape(local_rows, local_heads, HEAD_SIZE), query_gain
        ),
        grid_positions,
    ).astype(jnp.bfloat16)
    query_matrix = jnp.transpose(query_rows, (1, 0, 2)).reshape(local_heads * local_rows, HEAD_SIZE)
    shared = tp_index * local_heads // queries_per_group
    own_keys = lax.dynamic_slice_in_dim(keys, shared * HEAD_SIZE, HEAD_SIZE, 1)
    own_values = lax.dynamic_slice_in_dim(values, shared * HEAD_SIZE, HEAD_SIZE, 1)
    key_matrix = apply_rotary(
        per_head_norm(own_keys.astype(jnp.float32)[:, None, :], key_norm_gain), grid_positions
    )[:, 0, :].astype(jnp.bfloat16)
    score_scale = HEAD_SIZE ** (-0.5)
    query_count = local_heads * local_rows
    start_state = (
        jnp.full((query_count,), -1e30, jnp.float32),
        jnp.zeros((query_count,), jnp.float32),
        jnp.zeros((query_count, HEAD_SIZE), jnp.float32),
    )
    key_piece, value_piece = sent_together((key_matrix, own_values), "sp", 0, 1)
    piece_rows = key_piece.shape[0]
    block_count = -(-piece_rows // 2048)
    while piece_rows % block_count:
        block_count += 1
    block_width = piece_rows // block_count

    def one_block(block_index, state_inner):
        running_max, running_sum, weighted = state_inner
        block_keys = lax.dynamic_slice_in_dim(key_piece, block_index * block_width, block_width, 0)
        block_values = lax.dynamic_slice_in_dim(
            value_piece, block_index * block_width, block_width, 0
        )
        scores = (
            jnp.dot(query_matrix, block_keys.T, preferred_element_type=jnp.float32) * score_scale
        )
        new_max = jnp.maximum(running_max, jnp.max(scores, axis=1))
        factor = jnp.exp(running_max - new_max)
        weights = jnp.exp(scores - new_max[:, None])
        running_sum = running_sum * factor + jnp.sum(weights, axis=1)
        weighted = weighted * factor[:, None] + jnp.dot(
            weights.astype(jnp.bfloat16), block_values, preferred_element_type=jnp.float32
        )
        return (new_max, running_sum, weighted)

    running_max, running_sum, weighted = lax.fori_loop(0, block_count, one_block, start_state)
    attended = (weighted / running_sum[:, None]).astype(jnp.bfloat16)
    attended = jnp.transpose(
        attended.reshape(local_heads, local_rows, HEAD_SIZE), (1, 0, 2)
    ).reshape(local_rows, local_heads * HEAD_SIZE)
    own_width = residual_in.shape[1]
    attended_full = gathered_copies(attended, "tp", 1)
    group_width = local_heads * HEAD_SIZE
    share = jnp.zeros((local_rows, own_width), jnp.float32)
    for group_index in range(tp_count):
        left_part = attended_full[:, group_index * group_width : (group_index + 1) * group_width]
        right_part = weight_cols[group_index * group_width : (group_index + 1) * group_width, :]
        term = jnp.dot(left_part, right_part, preferred_element_type=jnp.float32).astype(
            jnp.bfloat16
        )
        share = share + term.astype(jnp.float32)
    residual_mid = residual_in.astype(jnp.float32) + share
    squares = taken_together(jnp.sum(residual_mid * residual_mid, axis=1), "tp")
    gain_own = lax.dynamic_slice_in_dim(mlp_gain, tp_index * own_width, own_width, 0)
    normed_own = (residual_mid * lax.rsqrt(squares / D + eps)[:, None] * gain_own).astype(
        jnp.bfloat16
    )
    normed = lax.all_gather(normed_own, "tp", axis=1, tiled=True)
    pieces = sent_together((gate_weight, up_weight), "sp", 0, 1)
    gate_out = jnp.dot(normed, pieces[0], preferred_element_type=jnp.float32)
    up_out = jnp.dot(normed, pieces[1], preferred_element_type=jnp.float32)
    hidden = (jax.nn.silu(gate_out) * up_out).astype(jnp.bfloat16)
    down_terms = jnp.dot(
        hidden,
        lax.all_gather(down_weight, "sp", axis=1, tiled=True),
        preferred_element_type=jnp.float32,
    )
    down_share = summed_on_arrival(down_terms.astype(jnp.bfloat16), "tp", 1)
    return (residual_mid + 0.5 * down_share).astype(jnp.bfloat16)


def solution(mesh):
    in_specs = (
        P("sp", "tp"),
        P("sp", "tp"),
        P("sp", None),
        P("sp", None),
        P(),
        P(),
        P("tp", None),
        P(),
        P("sp", "tp"),
        P("sp", "tp"),
        P("tp", "sp"),
    )
    out_specs = P("sp", "tp")
    return jax.shard_map(
        on_device, mesh=mesh, in_specs=in_specs, out_specs=out_specs, check_vma=False
    )
```

profile of v0, /device:TPU:1, one launch (start us, length us, event | category | flops | bytes accessed | tf_op | source)
XLA Modules:
  0.0 336.8 jit_solution(7837900333065985362)
XLA Ops:
  14.6 5.8 %all-to-all-start.1 = ((bf16[128,8,256]{0,2,1:T(8,128)(2,1)}), bf16[128,8,256]{0,2,1:T(8,128)(2,1)S(1)}, u32[]{:S(2)}, u32[]{:S(2)}) async-start(bf16[128,8,256]{0,2,1:T(8,128)(2,1)} %bitcast.9), calls=%async_computation.1 | async-start | bytes 1048576 | tf_op jit(solution)/shard_map/all_to_all | solution.py:100
  21.4 56.8 %all-gather.5.cloned.1.call-done = bf16[12288,256]{1,0:T(8,128)(2,1)} async-done(((bf16[768,256]{1,0:T(8,128)(2,1)}), bf16[12288,256]{1,0:T(8,128)(2,1)}) %all-gather.5.cloned.1.call-update) | async-done | bytes 6291472 | tf_op jit(solution)/shard_map/all_gather | solution.py:21
  78.2 4.7 %fusion.66 = (bf16[12288,128]{1,0:T(8,128)(2,1)}, bf16[12288,128]{1,0:T(8,128)(2,1)}) fusion(bf16[12288,256]{1,0:T(8,128)(2,1)} %all-gather.5.cloned.1.call-done), kind=kLoop, calls=%fused_computation.114 | loop fusion | bytes 12582912 | tf_op jit(solution)/shard_map/split | solution.py:21
  82.9 71.6 %while.18 = (s32[]{:T(128)}, f32[768]{0:T(1024)S(1)}, f32[768]{0:T(1024)S(1)}, f32[768,128]{1,0:T(8,128)S(1)}, bf16[12288,128]{1,0:T(8,128)(2,1)}, /*index=5*/bf...) while((s32[]{:T(128)}, f32[768]{0:T(1024)S(1)}, ...), condition=%wide.region_5.6_spmd.clone, body=%wide.region_2.5_spmd.clone.sunk | while | flops 818188032 | bytes 46121160 | solution.py:146
  82.9 4.7 %multiply_reduce_fusion.3 = (f32[768]{0:T(1024)S(1)}, f32[2048,768]{1,0:T(8,128)}) fusion(bf16[768,128]{1,0:T(8,128)(2,1)S(1)} %get-tuple-element.268, bf16[12288,128]{1,0:T(8,128)(2,1)} %get-tuple-element.267, s32[]{:T(128)S(6)} %select_n.55), kind=kOutput, calls=%fused_computation.1.clone.1 | convolution fusion | flops 405798144 | bytes 7015428 | tf_op jit(solution)/shard_map/while/body/eval_jaxpr/dot_general | solution.py:135
  87.6 4.2 %fusion.80 = f32[768]{0:T(1024)S(1)} fusion(f32[2048,768]{1,0:T(8,128)} %get-tuple-element.238, f32[768]{0:T(1024)S(1)} %select_maximum_fusion.2), kind=kLoop, calls=%fused_computation.3.clone.1 | loop fusion | flops 4717824 | bytes 6297600 | tf_op jit(solution)/shard_map/while/body/eval_jaxpr/reduce_sum | solution.py:140
  92.6 2.4 fusion.82
  95.0 4.7 %multiply_reduce_fusion.3 = (f32[768]{0:T(1024)S(1)}, f32[2048,768]{1,0:T(8,128)}) fusion(bf16[768,128]{1,0:T(8,128)(2,1)S(1)} %get-tuple-element.268, bf16[12288,128]{1,0:T(8,128)(2,1)} %get-tuple-element.267, s32[]{:T(128)S(6)} %select_n.55), kind=kOutput, calls=%fused_computation.1.clone.1 | convolution fusion | flops 405798144 | bytes 7015428 | tf_op jit(solution)/shard_map/while/body/eval_jaxpr/dot_general | solution.py:135
  99.6 4.1 %fusion.80 = f32[768]{0:T(1024)S(1)} fusion(f32[2048,768]{1,0:T(8,128)} %get-tuple-element.238, f32[768]{0:T(1024)S(1)} %select_maximum_fusion.2), kind=kLoop, calls=%fused_computation.3.clone.1 | loop fusion | flops 4717824 | bytes 6297600 | tf_op jit(solution)/shard_map/while/body/eval_jaxpr/reduce_sum | solution.py:140
  104.3 2.4 fusion.82
  106.7 4.7 %multiply_reduce_fusion.3 = (f32[768]{0:T(1024)S(1)}, f32[2048,768]{1,0:T(8,128)}) fusion(bf16[768,128]{1,0:T(8,128)(2,1)S(1)} %get-tuple-element.268, bf16[12288,128]{1,0:T(8,128)(2,1)} %get-tuple-element.267, s32[]{:T(128)S(6)} %select_n.55), kind=kOutput, calls=%fused_computation.1.clone.1 | convolution fusion | flops 405798144 | bytes 7015428 | tf_op jit(solution)/shard_map/while/body/eval_jaxpr/dot_general | solution.py:135
  111.4 4.2 %fusion.80 = f32[768]{0:T(1024)S(1)} fusion(f32[2048,768]{1,0:T(8,128)} %get-tuple-element.238, f32[768]{0:T(1024)S(1)} %select_maximum_fusion.2), kind=kLoop, calls=%fused_computation.3.clone.1 | loop fusion | flops 4717824 | bytes 6297600 | tf_op jit(solution)/shard_map/while/body/eval_jaxpr/reduce_sum | solution.py:140
  116.4 2.4 fusion.82
  118.8 4.7 %multiply_reduce_fusion.3 = (f32[768]{0:T(1024)S(1)}, f32[2048,768]{1,0:T(8,128)}) fusion(bf16[768,128]{1,0:T(8,128)(2,1)S(1)} %get-tuple-element.268, bf16[12288,128]{1,0:T(8,128)(2,1)} %get-tuple-element.267, s32[]{:T(128)S(6)} %select_n.55), kind=kOutput, calls=%fused_computation.1.clone.1 | convolution fusion | flops 405798144 | bytes 7015428 | tf_op jit(solution)/shard_map/while/body/eval_jaxpr/dot_general | solution.py:135
  123.5 4.2 %fusion.80 = f32[768]{0:T(1024)S(1)} fusion(f32[2048,768]{1,0:T(8,128)} %get-tuple-element.238, f32[768]{0:T(1024)S(1)} %select_maximum_fusion.2), kind=kLoop, calls=%fused_computation.3.clone.1 | loop fusion | flops 4717824 | bytes 6297600 | tf_op jit(solution)/shard_map/while/body/eval_jaxpr/reduce_sum | solution.py:140
  128.5 2.4 fusion.82
  130.9 4.7 %multiply_reduce_fusion.3 = (f32[768]{0:T(1024)S(1)}, f32[2048,768]{1,0:T(8,128)}) fusion(bf16[768,128]{1,0:T(8,128)(2,1)S(1)} %get-tuple-element.268, bf16[12288,128]{1,0:T(8,128)(2,1)} %get-tuple-element.267, s32[]{:T(128)S(6)} %select_n.55), kind=kOutput, calls=%fused_computation.1.clone.1 | convolution fusion | flops 405798144 | bytes 7015428 | tf_op jit(solution)/shard_map/while/body/eval_jaxpr/dot_general | solution.py:135
  135.6 4.2 %fusion.80 = f32[768]{0:T(1024)S(1)} fusion(f32[2048,768]{1,0:T(8,128)} %get-tuple-element.238, f32[768]{0:T(1024)S(1)} %select_maximum_fusion.2), kind=kLoop, calls=%fused_computation.3.clone.1 | loop fusion | flops 4717824 | bytes 6297600 | tf_op jit(solution)/shard_map/while/body/eval_jaxpr/reduce_sum | solution.py:140
  140.5 2.4 fusion.82
  142.9 4.7 %multiply_reduce_fusion.3 = (f32[768]{0:T(1024)S(1)}, f32[2048,768]{1,0:T(8,128)}) fusion(bf16[768,128]{1,0:T(8,128)(2,1)S(1)} %get-tuple-element.268, bf16[12288,128]{1,0:T(8,128)(2,1)} %get-tuple-element.267, s32[]{:T(128)S(6)} %select_n.55), kind=kOutput, calls=%fused_computation.1.clone.1 | convolution fusion | flops 405798144 | bytes 7015428 | tf_op jit(solution)/shard_map/while/body/eval_jaxpr/dot_general | solution.py:135
  147.5 4.0 %fusion.80 = f32[768]{0:T(1024)S(1)} fusion(f32[2048,768]{1,0:T(8,128)} %get-tuple-element.238, f32[768]{0:T(1024)S(1)} %select_maximum_fusion.2), kind=kLoop, calls=%fused_computation.3.clone.1 | loop fusion | flops 4717824 | bytes 6297600 | tf_op jit(solution)/shard_map/while/body/eval_jaxpr/reduce_sum | solution.py:140
  152.1 2.4 fusion.82
  156.2 5.2 %all-to-all-start = ((bf16[8,768,128]{1,2,0:T(8,128)(2,1)}), bf16[8,768,128]{1,2,0:T(8,128)(2,1)S(1)}, u32[]{:S(2)}, u32[]{:S(2)}) async-start(bf16[8,768,128]{1,2,0:T(8,128)(2,1)} %broadcast_in_dim.17), calls=%async_computation | async-start | bytes 3145728 | tf_op jit(solution)/shard_map/all_to_all | solution.py:32
  163.3 18.7 %all-to-all-done = bf16[8,768,128]{1,2,0:T(8,128)(2,1)S(1)} async-done(((bf16[8,768,128]{1,2,0:T(8,128)(2,1)}), bf16[8,768,128]{1,2,0:T(8,128)(2,1)S(1)}, u32[]{:S(2)}, u32[]{:S(2)}) %all-to-all-start) | async-done | bytes 1572896 | tf_op jit(solution)/shard_map/all_to_all | solution.py:32
  184.9 4.2 %all-to-all-start.2 = ((f32[8,1,768]{2,1,0:T(1,128)}), f32[8,1,768]{2,1,0:T(1,128)S(1)}, u32[]{:S(2)}, u32[]{:S(2)}) async-start(f32[8,1,768]{2,1,0:T(1,128)} %broadcast_in_dim.18), calls=%async_computation.2 | async-start | bytes 49152 | tf_op jit(solution)/shard_map/all_to_all | solution.py:32
  189.9 3.9 %all-to-all-done.2 = f32[8,1,768]{2,1,0:T(1,128)S(1)} async-done(((f32[8,1,768]{2,1,0:T(1,128)}), f32[8,1,768]{2,1,0:T(1,128)S(1)}, u32[]{:S(2)}, u32[]{:S(2)}) %all-to-all-start.2) | async-done | bytes 24608 | tf_op jit(solution)/shard_map/all_to_all | solution.py:32
  195.3 24.9 %all-gather.7.cloned.1.call-done = bf16[768,2048]{0,1:T(8,128)(2,1)} async-done(((bf16[768,256]{0,1:T(8,128)(2,1)}), bf16[768,2048]{0,1:T(8,128)(2,1)}) %all-gather.7.cloned.1.call-update) | async-done | bytes 3145744 | tf_op jit(solution)/shard_map/all_gather | solution.py:168
  220.2 5.2 %fusion.16 = f32[768,704]{0,1:T(8,128)S(1)} fusion(bf16[768,2048]{0,1:T(8,128)(2,1)} %all-gather.7.cloned.1.call-done, bf16[2048,1408]{0,1:T(8,128)(2,1)} %all-gather.9.cloned.1.call-done), kind=kOutput, calls=%fused_computation.22 | convolution fusion | flops 2214592512 | bytes 8192000 | tf_op jit(solution)/shard_map/dot_general | solution.py:170
  225.4 45.8 %all-gather.11.cloned.1.call-done = bf16[704,2048]{1,0:T(8,128)(2,1)} async-done(((bf16[704,128]{1,0:T(8,128)(2,1)}), bf16[704,2048]{1,0:T(8,128)(2,1)}) %all-gather.11.cloned.1.call-update) | async-done | bytes 2883600 | tf_op jit(solution)/shard_map/all_gather | solution.py:175
  271.2 11.7 %convolution_convert_fusion = bf16[768,2048]{1,0:T(8,128)(2,1)} fusion(bf16[704,2048]{1,0:T(8,128)(2,1)} %all-gather.11.cloned.1.call-done, f32[768,704]{0,1:T(8,128)S(1)} %fusion.16, bf16[768,2048]{0,1:T(8,128)(2,1)} %all-gather.7.cloned.1.call-done, bf16[2048,1408]{0,1:T(8,128)(2,1)} %all-gather.9.cloned.1.call-done), kind=kOutput, calls=%fused_computation.18 | convolution fusion | flops 4434001920 | bytes 14221312 | tf_op jit(solution)/shard_map/dot_general | solution.py:173
  282.9 2.1 copy.79
  285.0 43.5 %all_to_all.32 = bf16[8,768,256]{2,1,0:T(8,128)(2,1)S(1)} all-to-all(bf16[8,768,256]{2,1,0:T(8,128)(2,1)S(1)} %bitcast.66), channel_id=1, replica_groups=mesh['sp'=16,'tp'=8] {'tp'}, dimensions={0} | all-to-all | bytes 6291456 | tf_op jit(solution)/shard_map/all_to_all | solution.py:52
  (90 shorter events, 23.5 us)
Async XLA Ops:
  6.5 2.4 copy-start
  6.5 71.7 %all-gather.5.cloned.1.call-start = ((), (), s32[]{:S(2)}) async-start(), calls=%async_computation.4 | async-start | bytes 6684672 | tf_op jit(solution)/shard_map/all_gather | solution.py:21
  10.5 3.1 copy-start.3
  12.3 8.1 %copy-start.4 = (bf16[128,704]{0,1:T(8,128)(2,1)S(1)}, bf16[128,704]{0,1:T(8,128)(2,1)}, u32[]{:S(2)}) copy-start(bf16[128,704]{0,1:T(8,128)(2,1)} %param.22) | copy-start | bytes 540676
  12.3 8.1 %copy-start.5 = (bf16[128,704]{0,1:T(8,128)(2,1)S(1)}, bf16[128,704]{0,1:T(8,128)(2,1)}, u32[]{:S(2)}) copy-start(bf16[128,704]{0,1:T(8,128)(2,1)} %param.21) | copy-start | bytes 540676
  14.6 140.2 %all-to-all-start.1 = ((bf16[128,8,256]{0,2,1:T(8,128)(2,1)}), bf16[128,8,256]{0,2,1:T(8,128)(2,1)S(1)}, u32[]{:S(2)}, u32[]{:S(2)}) async-start(bf16[128,8,256]{0,2,1:T(8,128)(2,1)} %bitcast.9), calls=%async_computation.1 | async-start | bytes 1048576 | tf_op jit(solution)/shard_map/all_to_all | solution.py:100
  20.4 174.9 %all-gather.9.cloned.1.call-start = ((), (), s32[]{:S(2)}) async-start(), calls=%async_computation.6 | async-start | bytes 6127616 | tf_op jit(solution)/shard_map/all_gather | solution.py:21
  87.6 5.0 %copy-start.1 = (f32[2048,768]{1,0:T(8,128)S(1)}, f32[2048,768]{1,0:T(8,128)}, u32[]{:S(2)}) copy-start(f32[2048,768]{1,0:T(8,128)} %get-tuple-element.238) | copy-start | bytes 18874372 | tf_op jit(solution)/shard_map/while
  99.6 4.7 %copy-start.1 = (f32[2048,768]{1,0:T(8,128)S(1)}, f32[2048,768]{1,0:T(8,128)}, u32[]{:S(2)}) copy-start(f32[2048,768]{1,0:T(8,128)} %get-tuple-element.238) | copy-start | bytes 18874372 | tf_op jit(solution)/shard_map/while
  111.4 5.0 %copy-start.1 = (f32[2048,768]{1,0:T(8,128)S(1)}, f32[2048,768]{1,0:T(8,128)}, u32[]{:S(2)}) copy-start(f32[2048,768]{1,0:T(8,128)} %get-tuple-element.238) | copy-start | bytes 18874372 | tf_op jit(solution)/shard_map/while
  123.5 5.0 %copy-start.1 = (f32[2048,768]{1,0:T(8,128)S(1)}, f32[2048,768]{1,0:T(8,128)}, u32[]{:S(2)}) copy-start(f32[2048,768]{1,0:T(8,128)} %get-tuple-element.238) | copy-start | bytes 18874372 | tf_op jit(solution)/shard_map/while
  135.6 4.9 %copy-start.1 = (f32[2048,768]{1,0:T(8,128)S(1)}, f32[2048,768]{1,0:T(8,128)}, u32[]{:S(2)}) copy-start(f32[2048,768]{1,0:T(8,128)} %get-tuple-element.238) | copy-start | bytes 18874372 | tf_op jit(solution)/shard_map/while
  147.5 4.6 %copy-start.1 = (f32[2048,768]{1,0:T(8,128)S(1)}, f32[2048,768]{1,0:T(8,128)}, u32[]{:S(2)}) copy-start(f32[2048,768]{1,0:T(8,128)} %get-tuple-element.238) | copy-start | bytes 18874372 | tf_op jit(solution)/shard_map/while
  156.2 25.8 %all-to-all-start = ((bf16[8,768,128]{1,2,0:T(8,128)(2,1)}), bf16[8,768,128]{1,2,0:T(8,128)(2,1)S(1)}, u32[]{:S(2)}, u32[]{:S(2)}) async-start(bf16[8,768,128]{1,2,0:T(8,128)(2,1)} %broadcast_in_dim.17), calls=%async_computation | async-start | bytes 3145728 | tf_op jit(solution)/shard_map/all_to_all | solution.py:32
  183.0 1.0 copy-start.2
  184.9 8.9 %all-to-all-start.2 = ((f32[8,1,768]{2,1,0:T(1,128)}), f32[8,1,768]{2,1,0:T(1,128)S(1)}, u32[]{:S(2)}, u32[]{:S(2)}) async-start(f32[8,1,768]{2,1,0:T(1,128)} %broadcast_in_dim.18), calls=%async_computation.2 | async-start | bytes 49152 | tf_op jit(solution)/shard_map/all_to_all | solution.py:32
  189.1 31.1 %all-gather.7.cloned.1.call-start = ((), (), s32[]{:S(2)}) async-start(), calls=%async_computation.5 | async-start | bytes 3538944 | tf_op jit(solution)/shard_map/all_gather | solution.py:168
  194.7 76.4 %all-gather.11.cloned.1.call-start = ((), (), s32[]{:S(2)}) async-start(), calls=%async_computation.7 | async-start | bytes 3063808 | tf_op jit(solution)/shard_map/all_gather | solution.py:175
Sparse Core Ops, SparseCore 0:
  13.7 64.4 all-gather.4
  80.3 62.8 all-gather.8
  194.9 25.3 all-gather.6
  222.2 48.9 all-gather.10
where the time goes:
time: 338 us; the launch traced here: 337 us
  waiting for transfers between devices  151 us (45%)
  matrix products  61.1 us (18%)
  blocking collectives  43.5 us (13%)
  other arithmetic  34.3 us (10%)
  local copies, waits for them, and re-layouts  18.2 us (5%)
  starting transfers between devices  15.5 us (5%)
  between operations  13.4 us (4%)
    all_gather x2, waiting for transfers between devices, sent_together(): lax.all_gather(both, axis, axis=dim, tiled=True)  56.8 us
    all_gather x1, waiting for transfers between devices, on_device(): lax.all_gather(down_weight, 'sp', axis=1, tiled=True)  45.8 us
    all_to_all x1, blocking collectives, summed_on_arrival(): lax.all_to_all(tiles, axis, split_axis=0, concat_axis=0, tiled=True)  43.5 us
    dot_general x6, matrix products, one_block(): jnp.dot(query_matrix, block_keys.T, preferred_element_type=jnp.float32)  28 us
    all_gather x1, waiting for transfers between devices, on_device(): normed = lax.all_gather(normed_own, 'tp', axis=1, tiled=True)  24.9 us
    reduce_sum x6, other arithmetic, one_block(): running_sum = running_sum * factor + jnp.sum(weights, axis=1)  24.8 us
    all_to_all x2, waiting for transfers between devices, sent_to_all(): lax.all_to_all(jnp.broadcast_to(x[None], (size, *x.shape)), axis, 0, 0, t...  22.6 us
    dot_general x6, matrix products, one_block(): jnp.dot(weights.astype(jnp.bfloat16), block_values, preferred_element_typ...  14.2 us
  transfers between devices with their start and end apart: 7, of which 5 were waited for; matrix products, arithmetic and copies ran while one was open for 26% of the time, Pallas kernels for 0%

commit v1 on v0

--- a/solution.py
+++ b/solution.py
@@ -170,10 +170,17 @@
     gate_out = jnp.dot(normed, pieces[0], preferred_element_type=jnp.float32)
     up_out = jnp.dot(normed, pieces[1], preferred_element_type=jnp.float32)
     hidden = (jax.nn.silu(gate_out) * up_out).astype(jnp.bfloat16)
+
+    def slices_fit(on_dim, page, mesh_ax):
+        return jnp.concatenate(
+            lax.all_to_all(
+                jnp.stack(tuple((page for _ in range(lax.psum(1, mesh_ax)))), 0), mesh_ax, 0, 0
+            ),
+            on_dim,
+        )
+
     down_terms = jnp.dot(
-        hidden,
-        lax.all_gather(down_weight, "sp", axis=1, tiled=True),
-        preferred_element_type=jnp.float32,
+        hidden, slices_fit(1, down_weight, "sp"), preferred_element_type=jnp.float32
     )
     down_share = summed_on_arrival(down_terms.astype(jnp.bfloat16), "tp", 1)
     return (residual_mid + 0.5 * down_share).astype(jnp.bfloat16)

time: 338 us -> 309 us (0.914)
  waiting for transfers between devices: 151 us -> 117 us
  starting transfers between devices: 15.5 us -> 19.9 us
    all_gather x1 -> x0, waiting for transfers between devices: 45.8 us -> none  [on_device(): lax.all_gather(down_weight, 'sp', axis=1, tiled=True)]
    all_to_all x0 -> x1, waiting for transfers between devices: none -> 18.9 us  [slices_fit(): lax.all_to_all(jnp.stack(tuple((page for _ in range(lax.psum(1, mesh_ax))...]
    all_gather x1, waiting for transfers between devices: 24.9 us -> 18.6 us  [on_device(): normed = lax.all_gather(normed_own, 'tp', axis=1, tiled=True)]
    all_to_all x0 -> x1, starting transfers between devices: none -> 4.67 us  [slices_fit(): lax.all_to_all(jnp.stack(tuple((page for _ in range(lax.psum(1, mesh_ax))...]
  transfers between devices with their start and end apart: 7 -> 7, of which waited for: 5 -> 5; matrix products, arithmetic and copies ran while one was open for 26% -> 29% of each run, Pallas kernels for 0% -> 0%
where the time goes in v1:
time: 309 us; the launch traced here: 308 us
  waiting for transfers between devices  117 us (38%)
  matrix products  61.2 us (20%)
  blocking collectives  41.7 us (13%)
  other arithmetic  34.3 us (11%)
  local copies, waits for them, and re-layouts  20.4 us (7%)
  starting transfers between devices  19.9 us (6%)
  between operations  13.4 us (4%)
    all_gather x2, waiting for transfers between devices, sent_together(): lax.all_gather(both, axis, axis=dim, tiled=True)  56.8 us
    all_to_all x1, blocking collectives, summed_on_arrival(): lax.all_to_all(tiles, axis, split_axis=0, concat_axis=0, tiled=True)  41.7 us
    dot_general x6, matrix products, one_block(): jnp.dot(query_matrix, block_keys.T, preferred_element_type=jnp.float32)  28 us
    reduce_sum x6, other arithmetic, one_block(): running_sum = running_sum * factor + jnp.sum(weights, axis=1)  24.8 us
    all_to_all x2, waiting for transfers between devices, sent_to_all(): lax.all_to_all(jnp.broadcast_to(x[None], (size, *x.shape)), axis, 0, 0, t...  22.6 us
    all_to_all x1, waiting for transfers between devices, slices_fit(): lax.all_to_all(jnp.stack(tuple((page for _ in range(lax.psum(1, mesh_ax))...  18.9 us
    all_gather x1, waiting for transfers between devices, on_device(): normed = lax.all_gather(normed_own, 'tp', axis=1, tiled=True)  18.6 us
    dot_general x6, matrix products, one_block(): jnp.dot(weights.astype(jnp.bfloat16), block_values, preferred_element_typ...  14.2 us
  transfers between devices with their start and end apart: 7, of which 5 were waited for; matrix products, arithmetic and copies ran while one was open for 29% of the time, Pallas kernels for 0%

profile of v1, /device:TPU:1, one launch (start us, length us, event | category | flops | bytes accessed | tf_op | source)
XLA Modules:
  0.0 308.1 jit_solution(12489241211388810813)
XLA Ops:
  14.6 5.8 %all-to-all-start.1 = ((bf16[128,8,256]{0,2,1:T(8,128)(2,1)}), bf16[128,8,256]{0,2,1:T(8,128)(2,1)S(1)}, u32[]{:S(2)}, u32[]{:S(2)}) async-start(bf16[128,8,256]{0,2,1:T(8,128)(2,1)} %bitcast.9), calls=%async_computation.1 | async-start | bytes 1048576 | tf_op jit(solution)/shard_map/all_to_all | solution.py:100
  21.4 56.8 %all-gather.4.cloned.1.call-done = bf16[12288,256]{1,0:T(8,128)(2,1)} async-done(((bf16[768,256]{1,0:T(8,128)(2,1)}), bf16[12288,256]{1,0:T(8,128)(2,1)}) %all-gather.4.cloned.1.call-update) | async-done | bytes 6291472 | tf_op jit(solution)/shard_map/all_gather | solution.py:21
  78.2 4.7 %fusion.68 = (bf16[12288,128]{1,0:T(8,128)(2,1)}, bf16[12288,128]{1,0:T(8,128)(2,1)}) fusion(bf16[12288,256]{1,0:T(8,128)(2,1)} %all-gather.4.cloned.1.call-done), kind=kLoop, calls=%fused_computation.116 | loop fusion | bytes 12582912 | tf_op jit(solution)/shard_map/split | solution.py:21
  82.9 71.6 %while.18 = (s32[]{:T(128)}, f32[768]{0:T(1024)S(1)}, f32[768]{0:T(1024)S(1)}, f32[768,128]{1,0:T(8,128)S(1)}, bf16[12288,128]{1,0:T(8,128)(2,1)}, /*index=5*/bf...) while((s32[]{:T(128)}, f32[768]{0:T(1024)S(1)}, ...), condition=%wide.region_5.6_spmd.clone, body=%wide.region_2.5_spmd.clone.sunk | while | flops 818188032 | bytes 46121160 | solution.py:146
  82.9 4.7 %multiply_reduce_fusion.3 = (f32[768]{0:T(1024)S(1)}, f32[2048,768]{1,0:T(8,128)}) fusion(bf16[768,128]{1,0:T(8,128)(2,1)S(1)} %get-tuple-element.268, bf16[12288,128]{1,0:T(8,128)(2,1)} %get-tuple-element.267, s32[]{:T(128)S(6)} %select_n.55), kind=kOutput, calls=%fused_computation.1.clone.1 | convolution fusion | flops 405798144 | bytes 7015428 | tf_op jit(solution)/shard_map/while/body/eval_jaxpr/dot_general | solution.py:135
  87.6 4.2 %fusion.82 = f32[768]{0:T(1024)S(1)} fusion(f32[2048,768]{1,0:T(8,128)} %get-tuple-element.238, f32[768]{0:T(1024)S(1)} %select_maximum_fusion.2), kind=kLoop, calls=%fused_computation.3.clone.1 | loop fusion | flops 4717824 | bytes 6297600 | tf_op jit(solution)/shard_map/while/body/eval_jaxpr/reduce_sum | solution.py:140
  92.6 2.4 fusion.84
  95.0 4.7 %multiply_reduce_fusion.3 = (f32[768]{0:T(1024)S(1)}, f32[2048,768]{1,0:T(8,128)}) fusion(bf16[768,128]{1,0:T(8,128)(2,1)S(1)} %get-tuple-element.268, bf16[12288,128]{1,0:T(8,128)(2,1)} %get-tuple-element.267, s32[]{:T(128)S(6)} %select_n.55), kind=kOutput, calls=%fused_computation.1.clone.1 | convolution fusion | flops 405798144 | bytes 7015428 | tf_op jit(solution)/shard_map/while/body/eval_jaxpr/dot_general | solution.py:135
  99.6 4.1 %fusion.82 = f32[768]{0:T(1024)S(1)} fusion(f32[2048,768]{1,0:T(8,128)} %get-tuple-element.238, f32[768]{0:T(1024)S(1)} %select_maximum_fusion.2), kind=kLoop, calls=%fused_computation.3.clone.1 | loop fusion | flops 4717824 | bytes 6297600 | tf_op jit(solution)/shard_map/while/body/eval_jaxpr/reduce_sum | solution.py:140
  104.3 2.4 fusion.84
  106.7 4.7 %multiply_reduce_fusion.3 = (f32[768]{0:T(1024)S(1)}, f32[2048,768]{1,0:T(8,128)}) fusion(bf16[768,128]{1,0:T(8,128)(2,1)S(1)} %get-tuple-element.268, bf16[12288,128]{1,0:T(8,128)(2,1)} %get-tuple-element.267, s32[]{:T(128)S(6)} %select_n.55), kind=kOutput, calls=%fused_computation.1.clone.1 | convolution fusion | flops 405798144 | bytes 7015428 | tf_op jit(solution)/shard_map/while/body/eval_jaxpr/dot_general | solution.py:135
  111.4 4.2 %fusion.82 = f32[768]{0:T(1024)S(1)} fusion(f32[2048,768]{1,0:T(8,128)} %get-tuple-element.238, f32[768]{0:T(1024)S(1)} %select_maximum_fusion.2), kind=kLoop, calls=%fused_computation.3.clone.1 | loop fusion | flops 4717824 | bytes 6297600 | tf_op jit(solution)/shard_map/while/body/eval_jaxpr/reduce_sum | solution.py:140
  116.4 2.4 fusion.84
  118.8 4.7 %multiply_reduce_fusion.3 = (f32[768]{0:T(1024)S(1)}, f32[2048,768]{1,0:T(8,128)}) fusion(bf16[768,128]{1,0:T(8,128)(2,1)S(1)} %get-tuple-element.268, bf16[12288,128]{1,0:T(8,128)(2,1)} %get-tuple-element.267, s32[]{:T(128)S(6)} %select_n.55), kind=kOutput, calls=%fused_computation.1.clone.1 | convolution fusion | flops 405798144 | bytes 7015428 | tf_op jit(solution)/shard_map/while/body/eval_jaxpr/dot_general | solution.py:135
  123.5 4.2 %fusion.82 = f32[768]{0:T(1024)S(1)} fusion(f32[2048,768]{1,0:T(8,128)} %get-tuple-element.238, f32[768]{0:T(1024)S(1)} %select_maximum_fusion.2), kind=kLoop, calls=%fused_computation.3.clone.1 | loop fusion | flops 4717824 | bytes 6297600 | tf_op jit(solution)/shard_map/while/body/eval_jaxpr/reduce_sum | solution.py:140
  128.5 2.4 fusion.84
  130.9 4.7 %multiply_reduce_fusion.3 = (f32[768]{0:T(1024)S(1)}, f32[2048,768]{1,0:T(8,128)}) fusion(bf16[768,128]{1,0:T(8,128)(2,1)S(1)} %get-tuple-element.268, bf16[12288,128]{1,0:T(8,128)(2,1)} %get-tuple-element.267, s32[]{:T(128)S(6)} %select_n.55), kind=kOutput, calls=%fused_computation.1.clone.1 | convolution fusion | flops 405798144 | bytes 7015428 | tf_op jit(solution)/shard_map/while/body/eval_jaxpr/dot_general | solution.py:135
  135.6 4.2 %fusion.82 = f32[768]{0:T(1024)S(1)} fusion(f32[2048,768]{1,0:T(8,128)} %get-tuple-element.238, f32[768]{0:T(1024)S(1)} %select_maximum_fusion.2), kind=kLoop, calls=%fused_computation.3.clone.1 | loop fusion | flops 4717824 | bytes 6297600 | tf_op jit(solution)/shard_map/while/body/eval_jaxpr/reduce_sum | solution.py:140
  140.5 2.4 fusion.84
  142.9 4.7 %multiply_reduce_fusion.3 = (f32[768]{0:T(1024)S(1)}, f32[2048,768]{1,0:T(8,128)}) fusion(bf16[768,128]{1,0:T(8,128)(2,1)S(1)} %get-tuple-element.268, bf16[12288,128]{1,0:T(8,128)(2,1)} %get-tuple-element.267, s32[]{:T(128)S(6)} %select_n.55), kind=kOutput, calls=%fused_computation.1.clone.1 | convolution fusion | flops 405798144 | bytes 7015428 | tf_op jit(solution)/shard_map/while/body/eval_jaxpr/dot_general | solution.py:135
  147.5 4.0 %fusion.82 = f32[768]{0:T(1024)S(1)} fusion(f32[2048,768]{1,0:T(8,128)} %get-tuple-element.238, f32[768]{0:T(1024)S(1)} %select_maximum_fusion.2), kind=kLoop, calls=%fused_computation.3.clone.1 | loop fusion | flops 4717824 | bytes 6297600 | tf_op jit(solution)/shard_map/while/body/eval_jaxpr/reduce_sum | solution.py:140
  152.1 2.4 fusion.84
  156.2 5.2 %all-to-all-start = ((bf16[8,768,128]{1,2,0:T(8,128)(2,1)}), bf16[8,768,128]{1,2,0:T(8,128)(2,1)S(1)}, u32[]{:S(2)}, u32[]{:S(2)}) async-start(bf16[8,768,128]{1,2,0:T(8,128)(2,1)} %broadcast_in_dim.17), calls=%async_computation | async-start | bytes 3145728 | tf_op jit(solution)/shard_map/all_to_all | solution.py:32
  163.3 18.7 %all-to-all-done = bf16[8,768,128]{1,2,0:T(8,128)(2,1)S(1)} async-done(((bf16[8,768,128]{1,2,0:T(8,128)(2,1)}), bf16[8,768,128]{1,2,0:T(8,128)(2,1)S(1)}, u32[]{:S(2)}, u32[]{:S(2)}) %all-to-all-start) | async-done | bytes 1572896 | tf_op jit(solution)/shard_map/all_to_all | solution.py:32
  184.9 4.2 %all-to-all-start.2 = ((f32[8,1,768]{2,1,0:T(1,128)}), f32[8,1,768]{2,1,0:T(1,128)S(1)}, u32[]{:S(2)}, u32[]{:S(2)}) async-start(f32[8,1,768]{2,1,0:T(1,128)} %broadcast_in_dim.18), calls=%async_computation.2 | async-start | bytes 49152 | tf_op jit(solution)/shard_map/all_to_all | solution.py:32
  189.9 3.9 %all-to-all-done.2 = f32[8,1,768]{2,1,0:T(1,128)S(1)} async-done(((f32[8,1,768]{2,1,0:T(1,128)}), f32[8,1,768]{2,1,0:T(1,128)S(1)}, u32[]{:S(2)}, u32[]{:S(2)}) %all-to-all-start.2) | async-done | bytes 24608 | tf_op jit(solution)/shard_map/all_to_all | solution.py:32
  196.9 4.7 %all-to-all-start.3 = ((bf16[16,704,128]{2,1,0:T(8,128)(2,1)}), bf16[16,704,128]{2,1,0:T(8,128)(2,1)}, u32[]{:S(2)}, u32[]{:S(2)}) async-start(bf16[16,704,128]{2,1,0:T(8,128)(2,1)} %stack.2), calls=%async_computation.3 | async-start | bytes 5767168 | tf_op jit(solution)/shard_map/all_to_all | solution.py:176
  201.6 18.6 %all-gather.6.cloned.1.call-done = bf16[768,2048]{0,1:T(8,128)(2,1)} async-done(((bf16[768,256]{0,1:T(8,128)(2,1)}), bf16[768,2048]{0,1:T(8,128)(2,1)}) %all-gather.6.cloned.1.call-update) | async-done | bytes 3145744 | tf_op jit(solution)/shard_map/all_gather | solution.py:168
  220.2 5.2 %fusion.18 = f32[768,704]{0,1:T(8,128)S(1)} fusion(bf16[768,2048]{0,1:T(8,128)(2,1)} %all-gather.6.cloned.1.call-done, bf16[2048,1408]{0,1:T(8,128)(2,1)} %all-gather.8.cloned.1.call-done), kind=kOutput, calls=%fused_computation.24 | convolution fusion | flops 2214592512 | bytes 8192000 | tf_op jit(solution)/shard_map/dot_general | solution.py:170
  225.4 18.9 %all-to-all-done.3 = bf16[16,704,128]{2,1,0:T(8,128)(2,1)} async-done(((bf16[16,704,128]{2,1,0:T(8,128)(2,1)}), bf16[16,704,128]{2,1,0:T(8,128)(2,1)}, u32[]{:S(2)}, u32[]{:S(2)}) %all-to-all-start.3) | async-done | bytes 2883616 | tf_op jit(solution)/shard_map/all_to_all | solution.py:176
  244.3 11.8 %convolution_convert_fusion = bf16[768,2048]{1,0:T(8,128)(2,1)} fusion(f32[768,704]{0,1:T(8,128)S(1)} %fusion.18, bf16[768,2048]{0,1:T(8,128)(2,1)} %all-gather.6.cloned.1.call-done, bf16[2048,1408]{0,1:T(8,128)(2,1)} %all-gather.8.cloned.1.call-done, bf16[16,704,128]{2,1,0:T(8,128)(2,1)} %all-to-all-done.3), kind=kOutput, calls=%fused_computation.18 | convolution fusion | flops 4434001920 | bytes 14221312 | tf_op jit(solution)/shard_map/dot_general | solution.py:182
  258.1 41.7 %all_to_all.37 = bf16[8,768,256]{2,1,0:T(8,128)(2,1)S(1)} all-to-all(bf16[8,768,256]{2,1,0:T(8,128)(2,1)S(1)} %bitcast.73), channel_id=1, replica_groups=mesh['sp'=16,'tp'=8] {'tp'}, dimensions={0} | all-to-all | bytes 6291456 | tf_op jit(solution)/shard_map/all_to_all | solution.py:52
  (92 shorter events, 27.2 us)
Async XLA Ops:
  6.5 2.4 copy-start
  6.5 71.7 %all-gather.4.cloned.1.call-start = ((), (), s32[]{:S(2)}) async-start(), calls=%async_computation.5 | async-start | bytes 6684672 | tf_op jit(solution)/shard_map/all_gather | solution.py:21
  10.5 3.1 %copy-start.3 = (bf16[128,2048]{1,0:T(8,128)(2,1)S(1)}, bf16[128,2048]{1,0:T(8,128)(2,1)}, u32[]{:S(2)}) copy-start(bf16[128,2048]{1,0:T(8,128)(2,1)} %param.19) | copy-start | bytes 1572868
  12.3 8.1 %copy-start.4 = (bf16[128,704]{0,1:T(8,128)(2,1)S(1)}, bf16[128,704]{0,1:T(8,128)(2,1)}, u32[]{:S(2)}) copy-start(bf16[128,704]{0,1:T(8,128)(2,1)} %param.22) | copy-start | bytes 540676
  12.3 8.1 %copy-start.5 = (bf16[128,704]{0,1:T(8,128)(2,1)S(1)}, bf16[128,704]{0,1:T(8,128)(2,1)}, u32[]{:S(2)}) copy-start(bf16[128,704]{0,1:T(8,128)(2,1)} %param.21) | copy-start | bytes 540676
  14.6 140.2 %all-to-all-start.1 = ((bf16[128,8,256]{0,2,1:T(8,128)(2,1)}), bf16[128,8,256]{0,2,1:T(8,128)(2,1)S(1)}, u32[]{:S(2)}, u32[]{:S(2)}) async-start(bf16[128,8,256]{0,2,1:T(8,128)(2,1)} %bitcast.9), calls=%async_computation.1 | async-start | bytes 1048576 | tf_op jit(solution)/shard_map/all_to_all | solution.py:100
  20.4 181.2 %all-gather.8.cloned.1.call-start = ((), (), s32[]{:S(2)}) async-start(), calls=%async_computation.7 | async-start | bytes 6127616 | tf_op jit(solution)/shard_map/all_gather | solution.py:21
  87.6 5.0 %copy-start.1 = (f32[2048,768]{1,0:T(8,128)S(1)}, f32[2048,768]{1,0:T(8,128)}, u32[]{:S(2)}) copy-start(f32[2048,768]{1,0:T(8,128)} %get-tuple-element.238) | copy-start | bytes 18874372 | tf_op jit(solution)/shard_map/while
  99.6 4.7 %copy-start.1 = (f32[2048,768]{1,0:T(8,128)S(1)}, f32[2048,768]{1,0:T(8,128)}, u32[]{:S(2)}) copy-start(f32[2048,768]{1,0:T(8,128)} %get-tuple-element.238) | copy-start | bytes 18874372 | tf_op jit(solution)/shard_map/while
  111.4 5.0 %copy-start.1 = (f32[2048,768]{1,0:T(8,128)S(1)}, f32[2048,768]{1,0:T(8,128)}, u32[]{:S(2)}) copy-start(f32[2048,768]{1,0:T(8,128)} %get-tuple-element.238) | copy-start | bytes 18874372 | tf_op jit(solution)/shard_map/while
  123.5 5.0 %copy-start.1 = (f32[2048,768]{1,0:T(8,128)S(1)}, f32[2048,768]{1,0:T(8,128)}, u32[]{:S(2)}) copy-start(f32[2048,768]{1,0:T(8,128)} %get-tuple-element.238) | copy-start | bytes 18874372 | tf_op jit(solution)/shard_map/while
  135.6 4.9 %copy-start.1 = (f32[2048,768]{1,0:T(8,128)S(1)}, f32[2048,768]{1,0:T(8,128)}, u32[]{:S(2)}) copy-start(f32[2048,768]{1,0:T(8,128)} %get-tuple-element.238) | copy-start | bytes 18874372 | tf_op jit(solution)/shard_map/while
  147.5 4.6 %copy-start.1 = (f32[2048,768]{1,0:T(8,128)S(1)}, f32[2048,768]{1,0:T(8,128)}, u32[]{:S(2)}) copy-start(f32[2048,768]{1,0:T(8,128)} %get-tuple-element.238) | copy-start | bytes 18874372 | tf_op jit(solution)/shard_map/while
  156.2 25.8 %all-to-all-start = ((bf16[8,768,128]{1,2,0:T(8,128)(2,1)}), bf16[8,768,128]{1,2,0:T(8,128)(2,1)S(1)}, u32[]{:S(2)}, u32[]{:S(2)}) async-start(bf16[8,768,128]{1,2,0:T(8,128)(2,1)} %broadcast_in_dim.17), calls=%async_computation | async-start | bytes 3145728 | tf_op jit(solution)/shard_map/all_to_all | solution.py:32
  183.0 1.0 copy-start.2
  183.5 11.2 %copy-start.6 = (bf16[704,128]{1,0:T(8,128)(2,1)S(1)}, bf16[704,128]{1,0:T(8,128)(2,1)}, u32[]{:S(2)}) copy-start(bf16[704,128]{1,0:T(8,128)(2,1)} %param.23) | copy-start | bytes 540676
  184.9 8.9 %all-to-all-start.2 = ((f32[8,1,768]{2,1,0:T(1,128)}), f32[8,1,768]{2,1,0:T(1,128)S(1)}, u32[]{:S(2)}, u32[]{:S(2)}) async-start(f32[8,1,768]{2,1,0:T(1,128)} %broadcast_in_dim.18), calls=%async_computation.2 | async-start | bytes 49152 | tf_op jit(solution)/shard_map/all_to_all | solution.py:32
  189.1 31.1 %all-gather.6.cloned.1.call-start = ((), (), s32[]{:S(2)}) async-start(), calls=%async_computation.6 | async-start | bytes 3538944 | tf_op jit(solution)/shard_map/all_gather | solution.py:168
  196.9 47.4 %all-to-all-start.3 = ((bf16[16,704,128]{2,1,0:T(8,128)(2,1)}), bf16[16,704,128]{2,1,0:T(8,128)(2,1)}, u32[]{:S(2)}, u32[]{:S(2)}) async-start(bf16[16,704,128]{2,1,0:T(8,128)(2,1)} %stack.2), calls=%async_computation.3 | async-start | bytes 5767168 | tf_op jit(solution)/shard_map/all_to_all | solution.py:176
Sparse Core Ops, SparseCore 0:
  13.7 64.4 all-gather.3
  80.3 62.8 all-gather.7
  194.9 25.3 all-gather.5
